TPU v7x, 32 devices: a whole 2x2x4 slice. The times are simulated.
32 devices in a mesh: ep: 8 (over z, x), tp: 4 (over y, core).
Axes of the slice: x: 2, y: 2, z: 4, core: 2. Of those that a mesh axis runs over, the one named last changes fastest.
Arguments:
- tokens: bfloat16 [128, 2048], P('ep'), may hold values from -6 to 6
- lengths: int32 [128], P('ep'), may hold values from 1 to 1024, as said below
- key_cache: bfloat16 [128, 1024, 8, 128], P('ep', None, 'tp'), may hold values from -200 to 200
- value_cache: bfloat16 [128, 1024, 8, 128], P('ep', None, 'tp'), may hold values from -6 to 6
- attn_gain: float32 [2048], replicated, may hold values from 0.1 to 1.9
- w_query: bfloat16 [2048, 8, 128], P(None, 'tp'), may hold values from -0.1875 to 0.1875
- w_key: bfloat16 [2048, 8, 128], P(None, 'tp'), may hold values from -0.15625 to 0.15625
- w_value: bfloat16 [2048, 8, 128], P(None, 'tp'), may hold values from -0.125 to 0.125
- mix_lambda: float32 [8], P('tp'), may hold values from 0.3 to 0.8
- head_gain: float32 [128], replicated, may hold values from 0.1 to 1.9
- w_out: bfloat16 [8, 128, 2048], P('tp'), may hold values from -2.5 to 2.5
- ffn_gain: float32 [2048], replicated, may hold values from 0.1 to 1.9
- w_gate: bfloat16 [8, 2048, 2048], P('ep', None, 'tp'), may hold values from -1 to 1
- w_up: bfloat16 [8, 2048, 2048], P('ep', None, 'tp'), may hold values from -1 to 1
- w_down: bfloat16 [8, 2048, 2048], P('ep', 'tp'), may hold values from -0.046875 to 0.046875
- routes: int32 [128, 4], P('ep'), may hold values from 0 to 7, all different within a row; in each aligned block of 16 rows (0 to 15, 16 to 31, ...) at most 16 rows name the same one
- route_weights: float32 [128, 4], P('ep'), may hold values from 0.1 to 1
Outputs:
- mixed: bfloat16 [128, 2048], P('ep', 'tp')
Inputs may be any that keep to these rules, and one draw needn't show every extreme that they name: `routes`: in each aligned block of 16 rows no expert is named by more than 16 entries, and one is named by exactly 16 in some block; each row names 4 different experts. `lengths`: some sequence has all 1024 positions valid.
All inputs are finite; a program needn't handle non-finite values.
Results may differ from a plain program's by a relative error of at most 0.02.
The roundings to bfloat16 on the way count: a program that leaves them out, or rounds other values in their place, can miss the bound.
Values may be sent and summed in bfloat16 or wider, within the bound.
A program may use at most 128 MiB of HBM per device.

v0:
```python
import jax
import jax.numpy as jnp
from jax import lax
from jax.sharding import PartitionSpec as P

epsilon = 1e-06
clamp_limit = 7.0
sigmoid_slope = 1.702
branch_scale = 0.2


def norm_rows(source, gain):
    wide = source.astype(jnp.float32)
    return wide * lax.rsqrt(jnp.mean(wide * wide, axis=-1, keepdims=True) + epsilon) * gain


def mixed_weights(scores, own_scores, mix_lambda):
    peak = jnp.maximum(jnp.max(scores, axis=-1), own_scores)
    weights = jnp.exp(scores - peak[..., None])
    own_weight = jnp.exp(own_scores - peak)
    denominator = jnp.sum(weights, axis=-1) + own_weight
    shares = weights / denominator[..., None]
    own_share = own_weight / denominator
    balance = mix_lambda[None, :]
    mix_weights = (shares[:, :, 0] - balance[..., None] * shares[:, :, 1]).astype(jnp.bfloat16)
    own_mixed = (own_share[:, :, 0] - balance * own_share[:, :, 1]).astype(jnp.bfloat16)
    return (mix_weights, own_mixed)


def per_device(
    tokens,
    lengths,
    key_cache,
    value_cache,
    attn_gain,
    w_query,
    w_key,
    w_value,
    mix_lambda,
    head_gain,
    w_out,
    ffn_gain,
    w_gate,
    w_up,
    w_down,
    routes,
    route_weights,
):
    seq_dev, model_width = tokens.shape
    group_heads = w_query.shape[1]
    head_width = w_query.shape[2]
    half_width = head_width // 2
    columns = group_heads * head_width
    cache_len = key_cache.shape[1]
    normed = norm_rows(tokens, attn_gain).astype(jnp.bfloat16)
    queries = (
        jnp.dot(normed, w_query.reshape(model_width, columns), preferred_element_type=jnp.float32)
        .astype(jnp.bfloat16)
        .reshape(seq_dev, group_heads, head_width)
    )
    key_new = (
        jnp.dot(normed, w_key.reshape(model_width, columns), preferred_element_type=jnp.float32)
        .astype(jnp.bfloat16)
        .reshape(seq_dev, group_heads, head_width)
    )
    value_new = (
        jnp.dot(normed, w_value.reshape(model_width, columns), preferred_element_type=jnp.float32)
        .astype(jnp.bfloat16)
        .reshape(seq_dev, group_heads, head_width)
    )
    halves = (lax.iota(jnp.int32, head_width) < half_width).astype(jnp.bfloat16)
    stacked_query = jnp.stack([queries * halves, queries * (1 - halves)], axis=2)
    score_scale = half_width ** (-0.5)
    own_scores = (
        jnp.einsum("shcd,shd->shc", stacked_query, key_new, preferred_element_type=jnp.float32)
        * score_scale
    )
    positions = lax.iota(jnp.int32, cache_len)
    live_mask = (positions[None, :] < lengths[:, None])[:, None, None, :]
    scores = (
        jnp.einsum("shcd,slhd->shcl", stacked_query, key_cache, preferred_element_type=jnp.float32)
        * score_scale
    )
    scores = jnp.where(live_mask, scores, -jnp.inf)
    mix_weights, own_mixed = mixed_weights(scores, own_scores, mix_lambda)
    heads_out = jnp.einsum(
        "shl,slhd->shd", mix_weights, value_cache, preferred_element_type=jnp.float32
    )
    heads_out = heads_out + own_mixed.astype(jnp.float32)[..., None] * value_new.astype(jnp.float32)
    normed_heads = (
        heads_out
        * lax.rsqrt(jnp.mean(heads_out * heads_out, axis=-1, keepdims=True) + epsilon)
        * head_gain
        * branch_scale
    ).astype(jnp.bfloat16)
    partial_value = jnp.dot(
        normed_heads.reshape(seq_dev, columns),
        w_out.reshape(columns, model_width),
        preferred_element_type=jnp.float32,
    )
    partial_value = lax.optimization_barrier(partial_value.astype(jnp.bfloat16)).astype(jnp.float32)
    attention = lax.psum(partial_value.astype(jnp.bfloat16), "tp").astype(jnp.float32)
    residual = (tokens.astype(jnp.float32) + attention).astype(jnp.bfloat16)
    normed_ffn = norm_rows(residual, ffn_gain).astype(jnp.bfloat16)
    experts = lax.axis_size("ep")
    top_count = routes.shape[1]
    capacity = 2 * seq_dev * top_count // experts
    entries = routes.reshape(-1)
    onehot = (entries[:, None] == lax.iota(jnp.int32, experts)[None, :]).astype(jnp.int32)
    entry_slot = jnp.sum((jnp.cumsum(onehot, axis=0) - onehot) * onehot, axis=-1)
    target = entries * capacity + entry_slot
    slot_ids = lax.iota(jnp.int32, experts * capacity)
    placing = (slot_ids[:, None] == target[None, :]).astype(jnp.bfloat16)
    repeated = jnp.repeat(normed_ffn, top_count, axis=0)
    outgoing = jnp.dot(placing, repeated, preferred_element_type=jnp.float32).astype(jnp.bfloat16)
    outgoing = outgoing.reshape(experts, capacity, model_width)
    block_cols = model_width // lax.axis_size("tp")
    own_block = lax.dynamic_slice_in_dim(outgoing, lax.axis_index("tp") * block_cols, block_cols, 2)
    arrived = lax.all_gather(
        lax.all_to_all(own_block, "ep", split_axis=0, concat_axis=0, tiled=True),
        "tp",
        axis=2,
        tiled=True,
    )
    sources, slot_count, _ = arrived.shape
    flat_rows = arrived.reshape(sources * slot_count, model_width)
    gate_value = jnp.minimum(
        jnp.dot(flat_rows, w_gate[0], preferred_element_type=jnp.float32), clamp_limit
    )
    up_value = jnp.clip(
        jnp.dot(flat_rows, w_up[0], preferred_element_type=jnp.float32), -clamp_limit, clamp_limit
    )
    activated = ((up_value + 1.0) * gate_value * jax.nn.sigmoid(sigmoid_slope * gate_value)).astype(
        jnp.bfloat16
    )
    pieces = jnp.dot(activated, w_down[0], preferred_element_type=jnp.float32)
    pieces = lax.optimization_barrier(pieces.astype(jnp.bfloat16)).astype(jnp.float32)
    summed = lax.psum_scatter(
        pieces.reshape(sources, slot_count, model_width).astype(jnp.bfloat16),
        "tp",
        scatter_dimension=2,
        tiled=True,
    )
    returned = lax.all_to_all(summed, "ep", split_axis=0, concat_axis=0, tiled=True)
    slice_width = returned.shape[2]
    returned = returned.reshape(experts * capacity, slice_width).astype(jnp.float32)
    chosen = (target.reshape(seq_dev, top_count)[..., None] == slot_ids[None, None, :]).astype(
        jnp.float32
    )
    combine = jnp.sum(route_weights[..., None] * chosen, axis=1)
    expert_sum = jnp.dot(combine, returned, precision=lax.Precision.HIGHEST)
    own_columns = lax.dynamic_slice_in_dim(
        residual, lax.axis_index("tp") * slice_width, slice_width, 1
    )
    return (own_columns.astype(jnp.float32) + expert_sum).astype(jnp.bfloat16)


def solution(mesh):
    placed = (
        P("ep", None),
        P("ep"),
        P("ep", None, "tp", None),
        P("ep", None, "tp", None),
        P(),
        P(None, "tp", None),
        P(None, "tp", None),
        P(None, "tp", None),
        P("tp"),
        P(),
        P("tp", None, None),
        P(),
        P("ep", None, "tp"),
        P("ep", None, "tp"),
        P("ep", "tp", None),
        P("ep", None),
        P("ep", None),
    )
    return jax.shard_map(
        per_device, mesh=mesh, in_specs=placed, out_specs=P("ep", "tp"), check_vma=False
    )
```

profile of v0, /device:TPU:0, one launch (start us, length us, event | category | flops | bytes accessed | tf_op | source)
XLA Modules:
  0.0 125.2 jit_solution(6556066839307545895)
XLA Ops:
  6.6 1.1 fusion.55
  7.7 1.6 %convolution_convert_fusion.4 = bf16[16,256]{1,0:T(8,128)(2,1)S(1)} fusion(bf16[256,8,2,128]{3,2,1,0:T(2,128)(2,1)} %bitcast.110, bf16[16,2048]{1,0:T(8,128)(2,1)} %param.17, f32[2048]{0:T(1024)} %param.21, f32[16]{0:T(128)S(1)} %add_rsqrt_fusion.2), kind=kOutput, calls=%fused_computation.26 | convolution fusion | flops 16912384 | bytes 1130560 | tf_op jit(solution)/shard_map/dot_general | solution.py:57
  9.3 1.6 %convolution_convert_fusion.3 = bf16[16,256]{1,0:T(8,128)(2,1)S(1)} fusion(bf16[256,8,2,128]{3,2,1,0:T(2,128)(2,1)} %bitcast.111, bf16[16,2048]{1,0:T(8,128)(2,1)} %param.17, f32[2048]{0:T(1024)} %param.21, f32[16]{0:T(128)S(1)} %add_rsqrt_fusion.2), kind=kOutput, calls=%fused_computation.25 | convolution fusion | flops 16912384 | bytes 1130560 | tf_op jit(solution)/shard_map/dot_general | solution.py:62
  11.0 0.1 fusion.90
  11.1 0.1 copy.68
  11.3 5.8 %fusion.89 = (f32[16,2,2]{2,1,0:T(2,128)S(1)}, f32[16,2,2,1024]{3,2,1,0:T(2,128)S(1)}) fusion(bf16[16,2,2,128]{3,2,1,0:T(2,128)(2,1)S(1)} %pad_maximum_fusion, bf16[16,1024,2,128]{3,2,1,0:T(2,128)(2,1)} %param.19, pred[16,1024]{1,0:T(8,128)(4,1)S(1)} %iota_compare_fusion.1), kind=kOutput, calls=%fused_computation.105 | convolution fusion | flops 16973760 | bytes 8683776 | tf_op jit(solution)/shard_map/shcd,slhd->shcl/dot_general | solution.py:81
  17.2 0.1 copy.59
  17.3 0.1 copy.60
  17.4 0.3 fusion.51
  17.7 0.1 copy.61
  17.8 0.1 copy.62
  17.9 0.3 fusion.50
  18.2 0.2 fusion.88
  18.5 0.3 fusion.35
  18.8 0.2 fusion.66
  19.1 4.8 %fusion = f32[16,2,1,128]{3,2,1,0:T(1,128)S(1)} fusion(bf16[16,1024,2,128]{3,2,1,0:T(2,128)(2,1)} %param.20, bf16[16,2,1024,1]{2,1,0,3:T(2,128)(2,1)S(1)} %fusion.66), kind=kOutput, calls=%fused_computation | convolution fusion | flops 8388608 | bytes 8470528 | tf_op jit(solution)/shard_map/shl,slhd->shd/dot_general | solution.py:86
  23.9 0.2 multiply_reduce_fusion
  24.1 0.9 fusion.4
  25.3 0.1 reduce_window_sum.11
  25.4 0.2 select_reduce_fusion.1
  25.6 33.8 %all-reduce.2.cloned.1.call-done = bf16[16,2048]{1,0:T(8,128)(2,1)} async-done(((bf16[16,2048]{1,0:T(8,128)(2,1)}), bf16[16,2048]{1,0:T(8,128)(2,1)}) %all-reduce.2.cloned.1.call-update) | async-done | bytes 65552 | tf_op jit(solution)/shard_map/psum | solution.py:102
  59.4 1.0 fusion.52
  60.5 0.1 broadcast_in_dim.16
  60.7 0.3 convolution_convert_fusion.1
  61.0 12.7 %all_to_all.10 = bf16[8,16,512]{2,1,0:T(8,128)(2,1)S(1)} all-to-all(bf16[8,16,512]{2,1,0:T(8,128)(2,1)S(1)} %constant_dynamic-slice_fusion), channel_id=1, replica_groups=mesh['ep'=8,'tp'=4] {'ep'}, dimensions={0} | all-to-all | bytes 262144 | tf_op jit(solution)/shard_map/all_to_all | solution.py:120
  73.6 6.5 %all_gather.3 = bf16[8,16,2048]{2,1,0:T(8,128)(2,1)S(1)} all-gather(bf16[8,16,512]{2,1,0:T(8,128)(2,1)S(1)} %all_to_all.10), channel_id=1, replica_groups=mesh['ep'=8,'tp'=4] {'tp'}, dimensions={2}, use_global_device_ids=true | all-gather | bytes 655360 | tf_op jit(solution)/shard_map/all_gather | solution.py:119
  80.1 2.0 %fusion.13 = f32[128,512]{1,0:T(8,128)S(1)} fusion(bf16[128,2048]{1,0:T(8,128)(2,1)S(1)} %bitcast.105, bf16[1,2048,512]{2,1,0:T(8,128)(2,1)} %param.29), kind=kOutput, calls=%fused_computation.14 | convolution fusion | flops 268500992 | bytes 2883584 | tf_op jit(solution)/shard_map/dot_general | solution.py:128
  82.2 3.2 %convolution_convert_fusion = bf16[128,2048]{1,0:T(8,128)(2,1)} fusion(bf16[1,512,2048]{2,1,0:T(8,128)(2,1)S(1)} %copy-done, f32[128,512]{1,0:T(8,128)S(1)} %fusion.13, bf16[128,2048]{1,0:T(8,128)(2,1)S(1)} %bitcast.106, bf16[1,2048,512]{2,1,0:T(8,128)(2,1)} %param.30), kind=kOutput, calls=%fused_computation.4 | convolution fusion | flops 537722880 | bytes 5505024 | tf_op jit(solution)/shard_map/dot_general | solution.py:136
  85.6 19.2 %reduce-scatter.2.cloned.1.call-done = bf16[8,16,512]{2,1,0:T(8,128)(2,1)} async-done(((bf16[8,16,2048]{2,1,0:T(8,128)(2,1)}), bf16[8,16,512]{2,1,0:T(8,128)(2,1)}) %reduce-scatter.2.cloned.1.call-update) | async-done | bytes 131088 | tf_op jit(solution)/shard_map/reduce_scatter | solution.py:138
  104.8 5.5 %all-to-all-start.1 = ((bf16[8,16,512]{2,1,0:T(8,128)(2,1)}), bf16[8,16,512]{2,1,0:T(8,128)(2,1)S(1)}, u32[]{:S(2)}, u32[]{:S(2)}) async-start(bf16[8,16,512]{2,1,0:T(8,128)(2,1)} %reduce-scatter.2.cloned.1.call-done), calls=%async_computation.2 | async-start | bytes 262144 | tf_op jit(solution)/shard_map/all_to_all | solution.py:144
  110.4 7.2 %all-to-all-done.1 = bf16[8,16,512]{2,1,0:T(8,128)(2,1)S(1)} async-done(((bf16[8,16,512]{2,1,0:T(8,128)(2,1)}), bf16[8,16,512]{2,1,0:T(8,128)(2,1)S(1)}, u32[]{:S(2)}, u32[]{:S(2)}) %all-to-all-start.1) | async-done | bytes 131104 | tf_op jit(solution)/shard_map/all_to_all | solution.py:144
  117.6 0.8 fusion.33
  (50 shorter events, 1.1 us)
Async XLA Ops:
  6.5 75.6 %copy-start = (bf16[1,512,2048]{2,1,0:T(8,128)(2,1)S(1)}, bf16[1,512,2048]{2,1,0:T(8,128)(2,1)}, u32[]{:S(2)}) copy-start(bf16[1,512,2048]{2,1,0:T(8,128)(2,1)} %param.31) | copy-start | bytes 6291460
  6.5 4.7 %copy-start.8 = (s32[16]{0:T(128)S(1)}, s32[16]{0:T(128)}, u32[]{:S(2)}) copy-start(s32[16]{0:T(128)} %param.18) | copy-start | bytes 196
  6.5 52.9 %all-reduce.2.cloned.1.call-start = ((), (), s32[]{:S(2)}) async-start(), calls=%async_computation.3 | async-start | bytes 131072 | tf_op jit(solution)/shard_map/psum | solution.py:102
  11.3 7.2 %copy-start.2 = (bf16[16,2048]{1,0:T(8,128)(2,1)S(1)}, bf16[16,2048]{1,0:T(8,128)(2,1)}, u32[]{:S(2)}) copy-start(bf16[16,2048]{1,0:T(8,128)(2,1)} %param.17) | copy-start | bytes 196612
  11.3 7.2 %copy-start.9 = (bf16[2048,2,128]{2,1,0:T(2,128)(2,1)S(1)}, bf16[2048,2,128]{2,1,0:T(2,128)(2,1)}, u32[]{:S(2)}) copy-start(bf16[2048,2,128]{2,1,0:T(2,128)(2,1)} %param.24) | copy-start | bytes 3145732
  11.3 7.2 %copy-start.10 = (f32[2048]{0:T(1024)S(1)}, f32[2048]{0:T(1024)}, u32[]{:S(2)}) copy-start(f32[2048]{0:T(1024)} %param.21) | copy-start | bytes 24580
  17.2 1.6 %copy-start.5 = (f32[2]{0:T(128)S(1)}, f32[2]{0:T(128)}, u32[]{:S(2)}) copy-start(f32[2]{0:T(128)} %param.25) | copy-start | bytes 28
  19.0 5.0 %copy-start.1 = (bf16[2,128,2048]{2,1,0:T(8,128)(2,1)S(1)}, bf16[2,128,2048]{2,1,0:T(8,128)(2,1)}, u32[]{:S(2)}) copy-start(bf16[2,128,2048]{2,1,0:T(8,128)(2,1)} %param.27) | copy-start | bytes 3145732
  19.0 5.0 %copy-start.7 = (f32[128]{0:T(128)S(1)}, f32[128]{0:T(128)}, u32[]{:S(2)}) copy-start(f32[128]{0:T(128)} %param.26) | copy-start | bytes 1540
  19.0 6.0 %copy-start.4 = (s32[16,4]{0,1:T(4,128)S(1)}, s32[16,4]{0,1:T(4,128)}, u32[]{:S(2)}) copy-start(s32[16,4]{0,1:T(4,128)} %param.32) | copy-start | bytes 772
  19.1 41.3 %copy-start.3 = (f32[2048]{0:T(1024)S(1)}, f32[2048]{0:T(1024)}, u32[]{:S(2)}) copy-start(f32[2048]{0:T(1024)} %param.28) | copy-start | bytes 24580
  25.0 79.8 %reduce-scatter.2.cloned.1.call-start = ((), (), s32[]{:S(2)}) async-start(), calls=%async_computation.4 | async-start | bytes 655360 | tf_op jit(solution)/shard_map/reduce_scatter | solution.py:138
  82.2 28.1 %copy-start.6 = (f32[16,4]{0,1:T(4,128)S(1)}, f32[16,4]{0,1:T(4,128)}, u32[]{:S(2)}) copy-start(f32[16,4]{0,1:T(4,128)} %param.33) | copy-start | bytes 772
  104.8 12.8 %all-to-all-start.1 = ((bf16[8,16,512]{2,1,0:T(8,128)(2,1)}), bf16[8,16,512]{2,1,0:T(8,128)(2,1)S(1)}, u32[]{:S(2)}, u32[]{:S(2)}) async-start(bf16[8,16,512]{2,1,0:T(8,128)(2,1)} %reduce-scatter.2.cloned.1.call-done), calls=%async_computation.2 | async-start | bytes 262144 | tf_op jit(solution)/shard_map/all_to_all | solution.py:144
Sparse Core Ops, SparseCore 0:
  25.1 34.2 all-reduce.1
  85.6 19.1 reduce-scatter.1
where the time goes:
time: 126 us; the launch traced here: 125 us
  waiting for transfers between devices  60.2 us (48%)
  matrix products  21.5 us (17%)
  blocking collectives  19.1 us (15%)
  between operations  13.7 us (11%)
  starting transfers between devices  5.55 us (4%)
  other arithmetic  3.87 us (3%)
  local copies, waits for them, and re-layouts  1.29 us (1%)
    psum x1, waiting for transfers between devices, per_device(): lax.psum(partial_value.astype(jnp.bfloat16), 'tp').astype(jnp.float32)  33.8 us
    reduce_scatter x1, waiting for transfers between devices, per_device(): lax.psum_scatter(pieces.reshape(sources, slot_count, model_width).astype(...  19.2 us
    all_to_all x1, blocking collectives, per_device(): lax.all_to_all(own_block, 'ep', split_axis=0, concat_axis=0, tiled=True)  12.7 us
    all_to_all x1, waiting for transfers between devices, per_device(): lax.all_to_all(summed, 'ep', split_axis=0, concat_axis=0, tiled=True)  7.24 us
    all_gather x1, blocking collectives, per_device(): lax.all_gather(lax.all_to_all(own_block, 'ep', split_axis=0, concat_axis=...  6.49 us
    dot_general x1, matrix products, per_device(): jnp.einsum('shcd,slhd->shcl', stacked_query, key_cache, preferred_element...  5.84 us
    all_to_all x1, starting transfers between devices, per_device(): lax.all_to_all(summed, 'ep', split_axis=0, concat_axis=0, tiled=True)  5.5 us
    dot_general x1, matrix products, per_device(): jnp.einsum('shl,slhd->shd', mix_weights, value_cache, preferred_element_t...  4.8 us
  transfers between devices with their start and end apart: 3, of which 3 were waited for; matrix products, arithmetic and copies ran while one was open for 1% of the time, Pallas kernels for 0%

commit v1 on v0

--- a/solution.py
+++ b/solution.py
@@ -1,6 +1,10 @@
+import functools
+
 import jax
 import jax.numpy as jnp
 from jax import lax
+from jax.experimental import pallas as pl
+from jax.experimental.pallas import tpu as pltpu
 from jax.sharding import PartitionSpec as P
 
 epsilon = 1e-06
@@ -25,6 +29,205 @@
     mix_weights = (shares[:, :, 0] - balance[..., None] * shares[:, :, 1]).astype(jnp.bfloat16)
     own_mixed = (own_share[:, :, 0] - balance * own_share[:, :, 1]).astype(jnp.bfloat16)
     return (mix_weights, own_mixed)
+
+
+MESH = pl.DeviceIdType.MESH
+
+
+def exchange_kernel(
+    n_ep,
+    n_tp,
+    heads_ref,
+    tokens_ref,
+    gain_ref,
+    routes_ref,
+    route_weights_ref,
+    w_out_hbm,
+    w_gate_hbm,
+    w_up_hbm,
+    w_down_hbm,
+    out_ref,
+    w_out_ref,
+    w_gate_ref,
+    w_up_ref,
+    w_down_ref,
+    part_ref,
+    part_in_ref,
+    rows_ref,
+    normed_ref,
+    piece_ref,
+    piece_in_ref,
+    weight_sems,
+    part_sems,
+    rows_sems,
+    piece_sems,
+):
+    my_ep, my_tp = lax.axis_index("ep"), lax.axis_index("tp")
+    n_all = n_ep * n_tp
+    me = my_ep * n_tp + my_tp
+    seq_dev = tokens_ref.shape[0]
+    block = out_ref.shape[1]
+
+    weight_pairs = (
+        (w_out_hbm, w_out_ref),
+        (w_gate_hbm, w_gate_ref),
+        (w_up_hbm, w_up_ref),
+        (w_down_hbm, w_down_ref),
+    )
+    weight_copies = [
+        pltpu.make_async_copy(source, target, weight_sems.at[i])
+        for i, (source, target) in enumerate(weight_pairs)
+    ]
+    for copy in weight_copies:
+        copy.start()
+
+    barrier = pltpu.get_barrier_semaphore()
+
+    def greet(k, carry):
+        peer = lax.rem(me + k, n_all)
+        pl.semaphore_signal(
+            barrier, inc=1, device_id=(peer // n_tp, lax.rem(peer, n_tp)), device_id_type=MESH
+        )
+        return carry
+
+    lax.fori_loop(1, n_all, greet, 0)
+
+    weight_copies[0].wait()
+    for c in range(n_tp):
+        columns = slice(c * block, (c + 1) * block)
+        part_ref[c] = jnp.dot(
+            heads_ref[...], w_out_ref[:, columns], preferred_element_type=jnp.float32
+        ).astype(jnp.bfloat16)
+    pl.semaphore_wait(barrier, n_all - 1)
+
+    for k in range(1, n_tp):
+        peer = lax.rem(my_tp + k, n_tp)
+        pltpu.make_async_remote_copy(
+            src_ref=part_ref.at[peer],
+            dst_ref=part_in_ref.at[k - 1],
+            send_sem=part_sems.at[0],
+            recv_sem=part_sems.at[1],
+            device_id=(my_ep, peer),
+            device_id_type=MESH,
+        ).start()
+    own_columns = pl.ds(pl.multiple_of(my_tp * block, block), block)
+    own_rows = pl.ds(pl.multiple_of(my_ep * seq_dev, seq_dev), seq_dev)
+    attention = part_ref[my_tp].astype(jnp.float32)
+    if n_tp > 1:
+        pltpu.make_async_copy(part_in_ref, part_in_ref, part_sems.at[1]).wait()
+        for k in range(1, n_tp):
+            attention += part_in_ref[k - 1].astype(jnp.float32)
+    residual = (tokens_ref[:, own_columns].astype(jnp.float32) + attention).astype(jnp.bfloat16)
+    rows_ref[own_rows, own_columns] = residual
+
+    def spread(k, carry):
+        peer = lax.rem(me + k, n_all)
+        pltpu.make_async_remote_copy(
+            src_ref=rows_ref.at[own_rows, own_columns],
+            dst_ref=rows_ref.at[own_rows, own_columns],
+            send_sem=rows_sems.at[0],
+            recv_sem=rows_sems.at[1],
+            device_id=(peer // n_tp, lax.rem(peer, n_tp)),
+            device_id_type=MESH,
+        ).start()
+        return carry
+
+    lax.fori_loop(1, n_all, spread, 0)
+    others = piece_in_ref.at[pl.ds(0, n_all - 1)]
+    pltpu.make_async_copy(others, others, rows_sems.at[1]).wait()
+    pltpu.make_async_copy(others, others, rows_sems.at[0]).wait()
+    wide = rows_ref[...].astype(jnp.float32)
+    scale = lax.rsqrt(jnp.mean(wide * wide, axis=-1, keepdims=True) + epsilon)
+    normed_ref[...] = (wide * scale * gain_ref[...]).astype(jnp.bfloat16)
+
+    weight_copies[1].wait()
+    gate_value = jnp.minimum(
+        jnp.dot(normed_ref[...], w_gate_ref[...], preferred_element_type=jnp.float32), clamp_limit
+    )
+    weight_copies[2].wait()
+    up_value = jnp.clip(
+        jnp.dot(normed_ref[...], w_up_ref[...], preferred_element_type=jnp.float32),
+        -clamp_limit,
+        clamp_limit,
+    )
+    activated = ((up_value + 1.0) * gate_value * jax.nn.sigmoid(sigmoid_slope * gate_value)).astype(
+        jnp.bfloat16
+    )
+    weight_copies[3].wait()
+
+    for c in range(n_tp):
+        columns = slice(c * block, (c + 1) * block)
+        piece = jnp.dot(
+            activated, w_down_ref[:, columns], preferred_element_type=jnp.float32
+        ).astype(jnp.bfloat16)
+        piece_ref[c] = piece.reshape(n_ep, seq_dev, block)
+
+        def hand_out(k, carry):
+            peer_ep = lax.rem(my_ep + k, n_ep)
+
+            @pl.when(jnp.logical_or(peer_ep != my_ep, c != my_tp))
+            def _():
+                pltpu.make_async_remote_copy(
+                    src_ref=piece_ref.at[c, peer_ep],
+                    dst_ref=piece_in_ref.at[me],
+                    send_sem=piece_sems.at[0],
+                    recv_sem=piece_sems.at[1],
+                    device_id=(peer_ep, c),
+                    device_id_type=MESH,
+                ).start()
+
+            return carry
+
+        lax.fori_loop(0, n_ep, hand_out, 0)
+    piece_in_ref[me] = piece_ref[my_tp, my_ep]
+    pltpu.make_async_copy(others, others, piece_sems.at[1]).wait()
+
+    total = rows_ref[own_rows, own_columns].astype(jnp.float32)
+    for expert in range(n_ep):
+        named = jnp.where(routes_ref[...] == expert, route_weights_ref[...], 0.0)
+        weight = jnp.sum(named, axis=1, keepdims=True)
+        summed = piece_in_ref[expert * n_tp].astype(jnp.float32)
+        for t in range(1, n_tp):
+            summed += piece_in_ref[expert * n_tp + t].astype(jnp.float32)
+        total += weight * summed.astype(jnp.bfloat16).astype(jnp.float32)
+    out_ref[...] = total.astype(jnp.bfloat16)
+    pltpu.make_async_copy(others, others, piece_sems.at[0]).wait()
+    if n_tp > 1:
+        pltpu.make_async_copy(part_in_ref, part_in_ref, part_sems.at[0]).wait()
+
+
+def exchange_layer(
+    heads, tokens, w_out, ffn_gain, routes, route_weights, w_gate, w_up, w_down
+):
+    n_ep, n_tp = lax.axis_size("ep"), lax.axis_size("tp")
+    seq_dev, model_width = tokens.shape
+    block = model_width // n_tp
+    vmem = pl.BlockSpec(memory_space=pltpu.VMEM)
+    anywhere = pl.BlockSpec(memory_space=pl.ANY)
+    bf16 = jnp.bfloat16
+    return pl.pallas_call(
+        functools.partial(exchange_kernel, n_ep, n_tp),
+        out_shape=jax.ShapeDtypeStruct((seq_dev, block), bf16),
+        in_specs=[vmem] * 5 + [anywhere] * 4,
+        out_specs=vmem,
+        scratch_shapes=[
+            pltpu.VMEM(w_out.shape, bf16),
+            pltpu.VMEM(w_gate.shape, bf16),
+            pltpu.VMEM(w_up.shape, bf16),
+            pltpu.VMEM(w_down.shape, bf16),
+            pltpu.VMEM((n_tp, seq_dev, block), bf16),
+            pltpu.VMEM((max(n_tp - 1, 1), seq_dev, block), bf16),
+            pltpu.VMEM((n_ep * seq_dev, model_width), bf16),
+            pltpu.VMEM((n_ep * seq_dev, model_width), bf16),
+            pltpu.VMEM((n_tp, n_ep, seq_dev, block), bf16),
+            pltpu.VMEM((n_ep * n_tp, seq_dev, block), bf16),
+            pltpu.SemaphoreType.DMA((4,)),
+            pltpu.SemaphoreType.DMA((2,)),
+            pltpu.SemaphoreType.DMA((2,)),
+            pltpu.SemaphoreType.DMA((2,)),
+        ],
+        compiler_params=pltpu.CompilerParams(collective_id=0, has_side_effects=True),
+    )(heads, tokens, ffn_gain, routes, route_weights, w_out, w_gate, w_up, w_down)
 
 
 def per_device(
@@ -93,66 +296,17 @@
         * head_gain
         * branch_scale
     ).astype(jnp.bfloat16)
-    partial_value = jnp.dot(
+    return exchange_layer(
         normed_heads.reshape(seq_dev, columns),
+        tokens,
         w_out.reshape(columns, model_width),
-        preferred_element_type=jnp.float32,
-    )
-    partial_value = lax.optimization_barrier(partial_value.astype(jnp.bfloat16)).astype(jnp.float32)
-    attention = lax.psum(partial_value.astype(jnp.bfloat16), "tp").astype(jnp.float32)
-    residual = (tokens.astype(jnp.float32) + attention).astype(jnp.bfloat16)
-    normed_ffn = norm_rows(residual, ffn_gain).astype(jnp.bfloat16)
-    experts = lax.axis_size("ep")
-    top_count = routes.shape[1]
-    capacity = 2 * seq_dev * top_count // experts
-    entries = routes.reshape(-1)
-    onehot = (entries[:, None] == lax.iota(jnp.int32, experts)[None, :]).astype(jnp.int32)
-    entry_slot = jnp.sum((jnp.cumsum(onehot, axis=0) - onehot) * onehot, axis=-1)
-    target = entries * capacity + entry_slot
-    slot_ids = lax.iota(jnp.int32, experts * capacity)
-    placing = (slot_ids[:, None] == target[None, :]).astype(jnp.bfloat16)
-    repeated = jnp.repeat(normed_ffn, top_count, axis=0)
-    outgoing = jnp.dot(placing, repeated, preferred_element_type=jnp.float32).astype(jnp.bfloat16)
-    outgoing = outgoing.reshape(experts, capacity, model_width)
-    block_cols = model_width // lax.axis_size("tp")
-    own_block = lax.dynamic_slice_in_dim(outgoing, lax.axis_index("tp") * block_cols, block_cols, 2)
-    arrived = lax.all_gather(
-        lax.all_to_all(own_block, "ep", split_axis=0, concat_axis=0, tiled=True),
-        "tp",
-        axis=2,
-        tiled=True,
-    )
-    sources, slot_count, _ = arrived.shape
-    flat_rows = arrived.reshape(sources * slot_count, model_width)
-    gate_value = jnp.minimum(
-        jnp.dot(flat_rows, w_gate[0], preferred_element_type=jnp.float32), clamp_limit
-    )
-    up_value = jnp.clip(
-        jnp.dot(flat_rows, w_up[0], preferred_element_type=jnp.float32), -clamp_limit, clamp_limit
-    )
-    activated = ((up_value + 1.0) * gate_value * jax.nn.sigmoid(sigmoid_slope * gate_value)).astype(
-        jnp.bfloat16
-    )
-    pieces = jnp.dot(activated, w_down[0], preferred_element_type=jnp.float32)
-    pieces = lax.optimization_barrier(pieces.astype(jnp.bfloat16)).astype(jnp.float32)
-    summed = lax.psum_scatter(
-        pieces.reshape(sources, slot_count, model_width).astype(jnp.bfloat16),
-        "tp",
-        scatter_dimension=2,
-        tiled=True,
-    )
-    returned = lax.all_to_all(summed, "ep", split_axis=0, concat_axis=0, tiled=True)
-    slice_width = returned.shape[2]
-    returned = returned.reshape(experts * capacity, slice_width).astype(jnp.float32)
-    chosen = (target.reshape(seq_dev, top_count)[..., None] == slot_ids[None, None, :]).astype(
-        jnp.float32
-    )
-    combine = jnp.sum(route_weights[..., None] * chosen, axis=1)
-    expert_sum = jnp.dot(combine, returned, precision=lax.Precision.HIGHEST)
-    own_columns = lax.dynamic_slice_in_dim(
-        residual, lax.axis_index("tp") * slice_width, slice_width, 1
-    )
-    return (own_columns.astype(jnp.float32) + expert_sum).astype(jnp.bfloat16)
+        ffn_gain.reshape(1, model_width),
+        routes,
+        route_weights,
+        w_gate[0],
+        w_up[0],
+        w_down[0],
+    )
 
 
 def solution(mesh):

time: 126 us -> 57.2 us (0.45)
  the two profiles are of different devices: /device:TPU:0 before, /device:TPU:5 now
where the time goes in v1:
time: 57.2 us; the launch traced here: 56.9 us
  Pallas kernels  35.4 us (62%)
  matrix products  14.2 us (25%)
  local copies, waits for them, and re-layouts  4.13 us (7%)
  other arithmetic  2.99 us (5%)
    pallas_call x1, Pallas kernels, exchange_layer(): pl.pallas_call(functools.partial(exchange_kernel, n_ep, n_tp), out_shape=...  35.4 us
    dot_general x1, matrix products, per_device(): jnp.einsum('shcd,slhd->shcl', stacked_query, key_cache, preferred_element...  5.83 us
    dot_general x1, matrix products, per_device(): jnp.einsum('shl,slhd->shd', mix_weights, value_cache, preferred_element_t...  4.75 us
    unnamed x18, local copies, waits for them, and re-layouts  3.32 us
    dot_general x1, matrix products, per_device(): jnp.dot(normed, w_query.reshape(model_width, columns), preferred_element_...  1.58 us
    dot_general x1, matrix products, per_device(): jnp.dot(normed, w_key.reshape(model_width, columns), preferred_element_ty...  1.57 us

profile of v1, /device:TPU:5, one launch (start us, length us, event | category | flops | bytes accessed | tf_op | source)
XLA Modules:
  0.0 56.9 jit_solution(5070171246217203075)
XLA Ops:
  0.0 1.0 %fusion.19 = f32[16]{0:T(128)S(1)} fusion(bf16[16,2048]{1,0:T(8,128)(2,1)} %tokens_ref.1), kind=kLoop, calls=%fused_computation.21 | loop fusion | flops 98288 | bytes 65600 | tf_op jit(solution)/shard_map/reduce_sum | solution.py:18
  1.0 1.6 %convolution_convert_fusion.2 = bf16[16,256]{1,0:T(8,128)(2,1)S(1)} fusion(bf16[256,8,2,128]{3,2,1,0:T(2,128)(2,1)} %bitcast.70, bf16[16,2048]{1,0:T(8,128)(2,1)} %tokens_ref.1, f32[2048]{0:T(1024)} %param.21, f32[16]{0:T(128)S(1)} %add_rsqrt_fusion.1), kind=kOutput, calls=%fused_computation.8 | convolution fusion | flops 16912384 | bytes 1130560 | tf_op jit(solution)/shard_map/dot_general | solution.py:260
  2.7 1.6 %convolution_convert_fusion.1 = bf16[16,256]{1,0:T(8,128)(2,1)S(1)} fusion(bf16[256,8,2,128]{3,2,1,0:T(2,128)(2,1)} %bitcast.71, bf16[16,2048]{1,0:T(8,128)(2,1)} %tokens_ref.1, f32[2048]{0:T(1024)} %param.21, f32[16]{0:T(128)S(1)} %add_rsqrt_fusion.1), kind=kOutput, calls=%fused_computation.7 | convolution fusion | flops 16912384 | bytes 1130560 | tf_op jit(solution)/shard_map/dot_general | solution.py:265
  4.3 0.2 fusion.36
  4.4 0.1 copy.47
  4.5 0.7 %iota_compare_fusion = pred[16,1024]{1,0:T(8,128)(4,1)S(1)} fusion(s32[16]{0:T(128)} %param.18), kind=kLoop, calls=%fused_computation.29 | loop fusion | flops 16384 | bytes 16448 | tf_op jit(solution)/shard_map/lt | solution.py:282
  5.3 0.0 copy-start
  5.3 0.0 copy-start.5
  5.3 0.0 copy-start.6
  5.3 0.0 copy-start.4
  5.3 0.0 copy-start.2
  5.4 5.8 %fusion.35 = (f32[16,2,2]{2,1,0:T(2,128)S(1)}, f32[16,2,2,1024]{3,2,1,0:T(2,128)S(1)}) fusion(bf16[16,2,2,128]{3,2,1,0:T(2,128)(2,1)S(1)} %pad_maximum_fusion, bf16[16,1024,2,128]{3,2,1,0:T(2,128)(2,1)} %param.19, pred[16,1024]{1,0:T(8,128)(4,1)S(1)} %iota_compare_fusion), kind=kOutput, calls=%fused_computation.52 | convolution fusion | flops 16973760 | bytes 8683776 | tf_op jit(solution)/shard_map/shcd,slhd->shcl/dot_general | solution.py:284
  11.2 0.1 copy.38
  11.3 0.1 copy.39
  11.4 0.4 fusion.18
  11.7 0.1 copy.40
  11.9 0.1 copy.41
  11.9 0.3 fusion.17
  12.2 0.2 fusion.34
  12.5 0.2 fusion.25
  12.6 4.7 %fusion = f32[16,2,1,128]{3,2,1,0:T(1,128)S(1)} fusion(bf16[16,1024,2,128]{3,2,1,0:T(2,128)(2,1)} %param.20, bf16[16,2,1024,1]{2,1,0,3:T(2,128)(2,1)S(1)} %fusion.25), kind=kOutput, calls=%fused_computation | convolution fusion | flops 8388608 | bytes 8470528 | tf_op jit(solution)/shard_map/shl,slhd->shd/dot_general | solution.py:289
  17.4 0.1 bitcast_convert_fusion
  17.5 0.1 copy.43
  17.5 0.0 copy-done.6
  17.6 0.3 fusion.7
  17.9 0.2 multiply_reduce_fusion
  18.1 0.1 multiply_convert_fusion
  18.2 0.6 %copy.92 = bf16[2,8,2,128]{3,1,2,0:T(8,128)(2,1)} copy(bf16[2,8,2,128]{3,2,1,0:T(2,128)(2,1)S(1)} %bitcast.68) | data formatting | bytes 16384
  18.8 0.7 %copy.44.routes_ref = s32[16,4]{1,0:T(8,128)} copy(s32[16,4]{0,1:T(4,128)S(1)} %copy-done.2) | data formatting | bytes 512 | tf_op args[15]
  19.5 0.7 %copy.45.route_weights_ref = f32[16,4]{1,0:T(8,128)} copy(f32[16,4]{0,1:T(4,128)S(1)} %copy-done.3) | data formatting | bytes 512 | tf_op args[16]
  20.1 35.4 %shard_map.163 = bf16[16,512]{1,0:T(8,128)(2,1)} custom-call(bf16[16,256]{1,0:T(8,128)(2,1)} %bitcast.67, bf16[16,2048]{1,0:T(8,128)(2,1)} %tokens_ref.1, f32[1,2048]{1,0:T(1,128)} %bitcast.69, s32[16,4]{1,0:T(8,128)} %copy.44.routes_ref, f32[16,4]{1,0:T(8,128)} %copy.45.route_weights_ref, bf16[256,2048]{1,0:T(8,128)(2,1)} %bitcast.64, ...), custom_call_target="tpu_custom_call" | custom-call | tf_op jit(solution)/shard_map/pallas_call | solution.py:208
  55.5 1.3 %copy.94 = bf16[16,512]{1,0:T(8,128)(2,1)} copy(bf16[16,512]{1,0:T(8,128)(2,1)} %shard_map.163) | data formatting | bytes 32768
  (19 shorter events, 0.2 us)
Async XLA Ops:
  0.0 12.5 %copy-start.1 = (f32[2]{0:T(128)S(1)}, f32[2]{0:T(128)}, u32[]{:S(2)}) copy-start(f32[2]{0:T(128)} %param.25) | copy-start | bytes 28
  5.3 12.3 %copy-start = (bf16[16,2048]{1,0:T(8,128)(2,1)S(1)}, bf16[16,2048]{1,0:T(8,128)(2,1)}, u32[]{:S(2)}) copy-start(bf16[16,2048]{1,0:T(8,128)(2,1)} %tokens_ref.1) | copy-start | bytes 196612
  5.3 12.3 %copy-start.5 = (bf16[2048,2,128]{2,1,0:T(2,128)(2,1)S(1)}, bf16[2048,2,128]{2,1,0:T(2,128)(2,1)}, u32[]{:S(2)}) copy-start(bf16[2048,2,128]{2,1,0:T(2,128)(2,1)} %param.24) | copy-start | bytes 3145732
  5.3 12.3 %copy-start.6 = (f32[2048]{0:T(1024)S(1)}, f32[2048]{0:T(1024)}, u32[]{:S(2)}) copy-start(f32[2048]{0:T(1024)} %param.21) | copy-start | bytes 24580
  5.3 12.7 %copy-start.4 = (f32[128]{0:T(128)S(1)}, f32[128]{0:T(128)}, u32[]{:S(2)}) copy-start(f32[128]{0:T(128)} %param.26) | copy-start | bytes 1540
  5.3 13.5 %copy-start.2 = (s32[16,4]{0,1:T(4,128)S(1)}, s32[16,4]{0,1:T(4,128)}, u32[]{:S(2)}) copy-start(s32[16,4]{0,1:T(4,128)} %param.32) | copy-start | bytes 772
  5.3 14.1 %copy-start.3 = (f32[16,4]{0,1:T(4,128)S(1)}, f32[16,4]{0,1:T(4,128)}, u32[]{:S(2)}) copy-start(f32[16,4]{0,1:T(4,128)} %param.33) | copy-start | bytes 772

commit v2 on v1

--- a/solution.py
+++ b/solution.py
@@ -57,14 +57,16 @@
     normed_ref,
     piece_ref,
     piece_in_ref,
+    back_ref,
+    back_in_ref,
     weight_sems,
     part_sems,
     rows_sems,
+    fan_sems,
     piece_sems,
+    back_sems,
 ):
     my_ep, my_tp = lax.axis_index("ep"), lax.axis_index("tp")
-    n_all = n_ep * n_tp
-    me = my_ep * n_tp + my_tp
     seq_dev = tokens_ref.shape[0]
     block = out_ref.shape[1]
 
@@ -83,14 +85,14 @@
 
     barrier = pltpu.get_barrier_semaphore()
 
-    def greet(k, carry):
-        peer = lax.rem(me + k, n_all)
+    for k in range(1, n_ep):
         pl.semaphore_signal(
-            barrier, inc=1, device_id=(peer // n_tp, lax.rem(peer, n_tp)), device_id_type=MESH
+            barrier, inc=1, device_id=(lax.rem(my_ep + k, n_ep), my_tp), device_id_type=MESH
         )
-        return carry
-
-    lax.fori_loop(1, n_all, greet, 0)
+    for k in range(1, n_tp):
+        pl.semaphore_signal(
+            barrier, inc=1, device_id=(my_ep, lax.rem(my_tp + k, n_tp)), device_id_type=MESH
+        )
 
     weight_copies[0].wait()
     for c in range(n_tp):
@@ -98,7 +100,7 @@
         part_ref[c] = jnp.dot(
             heads_ref[...], w_out_ref[:, columns], preferred_element_type=jnp.float32
         ).astype(jnp.bfloat16)
-    pl.semaphore_wait(barrier, n_all - 1)
+    pl.semaphore_wait(barrier, n_ep + n_tp - 2)
 
     for k in range(1, n_tp):
         peer = lax.rem(my_tp + k, n_tp)
@@ -120,22 +122,32 @@
     residual = (tokens_ref[:, own_columns].astype(jnp.float32) + attention).astype(jnp.bfloat16)
     rows_ref[own_rows, own_columns] = residual
 
-    def spread(k, carry):
-        peer = lax.rem(me + k, n_all)
-        pltpu.make_async_remote_copy(
-            src_ref=rows_ref.at[own_rows, own_columns],
-            dst_ref=rows_ref.at[own_rows, own_columns],
-            send_sem=rows_sems.at[0],
-            recv_sem=rows_sems.at[1],
-            device_id=(peer // n_tp, lax.rem(peer, n_tp)),
+    far_first = sorted(range(1, n_ep), key=lambda k: -min(k, n_ep - k))
+
+    def rows_copy(source_ep, device, sems, recv):
+        place = rows_ref.at[
+            pl.ds(pl.multiple_of(source_ep * seq_dev, seq_dev), seq_dev), own_columns
+        ]
+        return pltpu.make_async_remote_copy(
+            src_ref=place,
+            dst_ref=place,
+            send_sem=sems.at[0],
+            recv_sem=sems.at[recv],
+            device_id=device,
             device_id_type=MESH,
-        ).start()
-        return carry
-
-    lax.fori_loop(1, n_all, spread, 0)
-    others = piece_in_ref.at[pl.ds(0, n_all - 1)]
-    pltpu.make_async_copy(others, others, rows_sems.at[1]).wait()
-    pltpu.make_async_copy(others, others, rows_sems.at[0]).wait()
+        )
+
+    for k in far_first:
+        rows_copy(my_ep, (lax.rem(my_ep + k, n_ep), my_tp), rows_sems, k).start()
+    for k in [0] + far_first[::-1]:
+        source_ep = lax.rem(my_ep + n_ep - k, n_ep)
+        if k:
+            rows_copy(source_ep, (my_ep, my_tp), rows_sems, k).wait_recv()
+        for j in range(1, n_tp):
+            peer = lax.rem(my_tp + j, n_tp)
+            rows_copy(source_ep, (my_ep, peer), fan_sems, 1).start()
+    if n_tp > 1:
+        pltpu.make_async_copy(piece_in_ref, piece_in_ref, fan_sems.at[1]).wait()
     wide = rows_ref[...].astype(jnp.float32)
     scale = lax.rsqrt(jnp.mean(wide * wide, axis=-1, keepdims=True) + epsilon)
     normed_ref[...] = (wide * scale * gain_ref[...]).astype(jnp.bfloat16)
@@ -155,45 +167,68 @@
     )
     weight_copies[3].wait()
 
-    for c in range(n_tp):
-        columns = slice(c * block, (c + 1) * block)
+    targets = far_first + [0]
+    for j in sorted(range(1, n_tp), key=lambda j: -min(j, n_tp - j)) + [0]:
+        peer = lax.rem(my_tp + j, n_tp)
+        columns = pl.ds(pl.multiple_of(peer * block, block), block)
         piece = jnp.dot(
             activated, w_down_ref[:, columns], preferred_element_type=jnp.float32
         ).astype(jnp.bfloat16)
-        piece_ref[c] = piece.reshape(n_ep, seq_dev, block)
-
-        def hand_out(k, carry):
-            peer_ep = lax.rem(my_ep + k, n_ep)
-
-            @pl.when(jnp.logical_or(peer_ep != my_ep, c != my_tp))
-            def _():
+        piece_ref[j] = piece.reshape(n_ep, seq_dev, block)
+        if j:
+            for k in targets:
+                target_ep = lax.rem(my_ep + k, n_ep)
                 pltpu.make_async_remote_copy(
-                    src_ref=piece_ref.at[c, peer_ep],
-                    dst_ref=piece_in_ref.at[me],
-                    send_sem=piece_sems.at[0],
-                    recv_sem=piece_sems.at[1],
-                    device_id=(peer_ep, c),
+                    src_ref=piece_ref.at[j, target_ep],
+                    dst_ref=piece_in_ref.at[target_ep, j - 1],
+                    send_sem=fan_sems.at[2],
+                    recv_sem=piece_sems.at[k],
+                    device_id=(my_ep, peer),
                     device_id_type=MESH,
                 ).start()
 
-            return carry
-
-        lax.fori_loop(0, n_ep, hand_out, 0)
-    piece_in_ref[me] = piece_ref[my_tp, my_ep]
-    pltpu.make_async_copy(others, others, piece_sems.at[1]).wait()
+    for k in targets:
+        target_ep = lax.rem(my_ep + k, n_ep)
+        summed = piece_ref[0, target_ep].astype(jnp.float32)
+        if n_tp > 1:
+            landed = piece_in_ref.at[target_ep]
+            pltpu.make_async_copy(landed, landed, piece_sems.at[k]).wait()
+            for j in range(1, n_tp):
+                summed += piece_in_ref[target_ep, j - 1].astype(jnp.float32)
+        back_ref[k] = summed.astype(jnp.bfloat16)
+        if k:
+            pltpu.make_async_remote_copy(
+                src_ref=back_ref.at[k],
+                dst_ref=back_in_ref.at[k - 1],
+                send_sem=back_sems.at[0],
+                recv_sem=back_sems.at[k],
+                device_id=(target_ep, my_tp),
+                device_id_type=MESH,
+            ).start()
 
     total = rows_ref[own_rows, own_columns].astype(jnp.float32)
-    for expert in range(n_ep):
+    eye = lax.broadcasted_iota(jnp.int32, (seq_dev, seq_dev), 0) == lax.broadcasted_iota(
+        jnp.int32, (seq_dev, seq_dev), 1
+    )
+    for k in [0] + far_first[::-1]:
+        expert = lax.rem(my_ep + n_ep - k, n_ep)
         named = jnp.where(routes_ref[...] == expert, route_weights_ref[...], 0.0)
-        weight = jnp.sum(named, axis=1, keepdims=True)
-        summed = piece_in_ref[expert * n_tp].astype(jnp.float32)
-        for t in range(1, n_tp):
-            summed += piece_in_ref[expert * n_tp + t].astype(jnp.float32)
-        total += weight * summed.astype(jnp.bfloat16).astype(jnp.float32)
+        weight = jnp.sum(named, axis=0, keepdims=True)
+        weight = jnp.sum(jnp.where(eye, weight, 0.0), axis=1, keepdims=True)
+        if k:
+            arrived = back_in_ref.at[k - 1]
+            pltpu.make_async_copy(arrived, arrived, back_sems.at[k]).wait()
+            total += weight * back_in_ref[k - 1].astype(jnp.float32)
+        else:
+            total += weight * back_ref[0].astype(jnp.float32)
     out_ref[...] = total.astype(jnp.bfloat16)
-    pltpu.make_async_copy(others, others, piece_sems.at[0]).wait()
+    if n_ep > 1:
+        pltpu.make_async_copy(back_in_ref, back_in_ref, rows_sems.at[0]).wait()
+        pltpu.make_async_copy(back_in_ref, back_in_ref, back_sems.at[0]).wait()
     if n_tp > 1:
         pltpu.make_async_copy(part_in_ref, part_in_ref, part_sems.at[0]).wait()
+        pltpu.make_async_copy(piece_in_ref, piece_in_ref, fan_sems.at[0]).wait()
+        pltpu.make_async_copy(piece_in_ref, piece_in_ref, fan_sems.at[2]).wait()
 
 
 def exchange_layer(
@@ -220,11 +255,15 @@
             pltpu.VMEM((n_ep * seq_dev, model_width), bf16),
             pltpu.VMEM((n_ep * seq_dev, model_width), bf16),
             pltpu.VMEM((n_tp, n_ep, seq_dev, block), bf16),
-            pltpu.VMEM((n_ep * n_tp, seq_dev, block), bf16),
+            pltpu.VMEM((n_ep, max(n_tp - 1, 1), seq_dev, block), bf16),
+            pltpu.VMEM((n_ep, seq_dev, block), bf16),
+            pltpu.VMEM((max(n_ep - 1, 1), seq_dev, block), bf16),
             pltpu.SemaphoreType.DMA((4,)),
             pltpu.SemaphoreType.DMA((2,)),
-            pltpu.SemaphoreType.DMA((2,)),
-            pltpu.SemaphoreType.DMA((2,)),
+            pltpu.SemaphoreType.DMA((n_ep,)),
+            pltpu.SemaphoreType.DMA((3,)),
+            pltpu.SemaphoreType.DMA((n_ep,)),
+            pltpu.SemaphoreType.DMA((n_ep,)),
         ],
         compiler_params=pltpu.CompilerParams(collective_id=0, has_side_effects=True),
     )(heads, tokens, ffn_gain, routes, route_weights, w_out, w_gate, w_up, w_down)
@@ -301,8 +340,8 @@
         tokens,
         w_out.reshape(columns, model_width),
         ffn_gain.reshape(1, model_width),
-        routes,
-        route_weights,
+        routes.T,
+        route_weights.T,
         w_gate[0],
         w_up[0],
         w_down[0],

time: 57.2 us -> 55 us (0.962)
  the two profiles are of different devices: /device:TPU:5 before, /device:TPU:0 now
where the time goes in v2:
time: 55 us; the launch traced here: 54.7 us
  Pallas kernels  34.6 us (63%)
  matrix products  14.2 us (26%)
  other arithmetic  3 us (5%)
  local copies, waits for them, and re-layouts  2.77 us (5%)
    pallas_call x1, Pallas kernels, exchange_layer(): pl.pallas_call(functools.partial(exchange_kernel, n_ep, n_tp), out_shape=...  34.6 us
    dot_general x1, matrix products, per_device(): jnp.einsum('shcd,slhd->shcl', stacked_query, key_cache, preferred_element...  5.83 us
    dot_general x1, matrix products, per_device(): jnp.einsum('shl,slhd->shd', mix_weights, value_cache, preferred_element_t...  4.75 us
    unnamed x12, local copies, waits for them, and re-layouts  1.96 us
    dot_general x1, matrix products, per_device(): jnp.dot(normed, w_query.reshape(model_width, columns), preferred_element_...  1.58 us
    dot_general x1, matrix products, per_device(): jnp.dot(normed, w_key.reshape(model_width, columns), preferred_element_ty...  1.57 us

profile of v2, /device:TPU:0, one launch (start us, length us, event | category | flops | bytes accessed | tf_op | source)
XLA Modules:
  0.0 54.7 jit_solution(4464681162423087200)
XLA Ops:
  0.0 1.0 %fusion.19 = f32[16]{0:T(128)S(1)} fusion(bf16[16,2048]{1,0:T(8,128)(2,1)} %tokens_ref.1), kind=kLoop, calls=%fused_computation.21 | loop fusion | flops 98288 | bytes 65600 | tf_op jit(solution)/shard_map/reduce_sum | solution.py:18
  1.0 1.6 %convolution_convert_fusion.2 = bf16[16,256]{1,0:T(8,128)(2,1)S(1)} fusion(bf16[256,8,2,128]{3,2,1,0:T(2,128)(2,1)} %bitcast.74, bf16[16,2048]{1,0:T(8,128)(2,1)} %tokens_ref.1, f32[2048]{0:T(1024)} %param.21, f32[16]{0:T(128)S(1)} %add_rsqrt_fusion.1), kind=kOutput, calls=%fused_computation.8 | convolution fusion | flops 16912384 | bytes 1130560 | tf_op jit(solution)/shard_map/dot_general | solution.py:299
  2.7 1.6 %convolution_convert_fusion.1 = bf16[16,256]{1,0:T(8,128)(2,1)S(1)} fusion(bf16[256,8,2,128]{3,2,1,0:T(2,128)(2,1)} %bitcast.75, bf16[16,2048]{1,0:T(8,128)(2,1)} %tokens_ref.1, f32[2048]{0:T(1024)} %param.21, f32[16]{0:T(128)S(1)} %add_rsqrt_fusion.1), kind=kOutput, calls=%fused_computation.7 | convolution fusion | flops 16912384 | bytes 1130560 | tf_op jit(solution)/shard_map/dot_general | solution.py:304
  4.3 0.2 fusion.36
  4.4 0.1 copy.41
  4.5 0.7 %iota_compare_fusion = pred[16,1024]{1,0:T(8,128)(4,1)S(1)} fusion(s32[16]{0:T(128)} %param.18), kind=kLoop, calls=%fused_computation.29 | loop fusion | flops 16384 | bytes 16448 | tf_op jit(solution)/shard_map/lt | solution.py:321
  5.3 0.0 copy-start
  5.3 0.0 copy-start.3
  5.3 0.0 copy-start.4
  5.3 0.0 copy-start.2
  5.3 5.8 %fusion.35 = (f32[16,2,2]{2,1,0:T(2,128)S(1)}, f32[16,2,2,1024]{3,2,1,0:T(2,128)S(1)}) fusion(bf16[16,2,2,128]{3,2,1,0:T(2,128)(2,1)S(1)} %pad_maximum_fusion, bf16[16,1024,2,128]{3,2,1,0:T(2,128)(2,1)} %param.19, pred[16,1024]{1,0:T(8,128)(4,1)S(1)} %iota_compare_fusion), kind=kOutput, calls=%fused_computation.52 | convolution fusion | flops 16973760 | bytes 8683776 | tf_op jit(solution)/shard_map/shcd,slhd->shcl/dot_general | solution.py:323
  11.2 0.1 copy.34
  11.3 0.1 copy.35
  11.4 0.4 fusion.18
  11.7 0.1 copy.36
  11.8 0.1 copy.37
  11.9 0.3 fusion.17
  12.2 0.2 fusion.34
  12.4 0.0 copy-done.1
  12.5 0.2 fusion.25
  12.6 4.7 %fusion = f32[16,2,1,128]{3,2,1,0:T(1,128)S(1)} fusion(bf16[16,1024,2,128]{3,2,1,0:T(2,128)(2,1)} %param.20, bf16[16,2,1024,1]{2,1,0,3:T(2,128)(2,1)S(1)} %fusion.25), kind=kOutput, calls=%fused_computation | convolution fusion | flops 8388608 | bytes 8470528 | tf_op jit(solution)/shard_map/shl,slhd->shd/dot_general | solution.py:328
  17.4 0.1 bitcast_convert_fusion
  17.4 0.1 copy.39
  17.5 0.0 copy-done
  17.5 0.0 copy-done.3
  17.5 0.0 copy-done.4
  17.6 0.3 fusion.7
  17.9 0.2 multiply_reduce_fusion
  18.1 0.1 multiply_convert_fusion
  18.2 0.6 %copy.86 = bf16[2,8,2,128]{3,1,2,0:T(8,128)(2,1)} copy(bf16[2,8,2,128]{3,2,1,0:T(2,128)(2,1)S(1)} %bitcast.70) | data formatting | bytes 16384
  18.8 34.6 %shard_map.163 = bf16[16,512]{1,0:T(8,128)(2,1)} custom-call(bf16[16,256]{1,0:T(8,128)(2,1)} %bitcast.69, bf16[16,2048]{1,0:T(8,128)(2,1)} %tokens_ref.1, f32[1,2048]{1,0:T(1,128)} %bitcast.71, s32[4,16]{1,0:T(4,128)} %bitcast.72, f32[4,16]{1,0:T(4,128)} %bitcast.73, bf16[256,2048]{1,0:T(8,128)(2,1)} %bitcast.66, bf16[2048,512]{1,0:T(8,128)(2,1)} %bitcast.63, ...), custom_call_target="tpu_custom_call" | custom-call | tf_op jit(solution)/shard_map/pallas_call | solution.py:243
  53.4 1.3 %copy.88 = bf16[16,512]{1,0:T(8,128)(2,1)} copy(bf16[16,512]{1,0:T(8,128)(2,1)} %shard_map.163) | data formatting | bytes 32768
  (13 shorter events, 0.2 us)
Async XLA Ops:
  0.0 12.4 %copy-start.1 = (f32[2]{0:T(128)S(1)}, f32[2]{0:T(128)}, u32[]{:S(2)}) copy-start(f32[2]{0:T(128)} %param.25) | copy-start | bytes 28
  5.3 12.2 %copy-start = (bf16[16,2048]{1,0:T(8,128)(2,1)S(1)}, bf16[16,2048]{1,0:T(8,128)(2,1)}, u32[]{:S(2)}) copy-start(bf16[16,2048]{1,0:T(8,128)(2,1)} %tokens_ref.1) | copy-start | bytes 196612
  5.3 12.2 %copy-start.3 = (bf16[2048,2,128]{2,1,0:T(2,128)(2,1)S(1)}, bf16[2048,2,128]{2,1,0:T(2,128)(2,1)}, u32[]{:S(2)}) copy-start(bf16[2048,2,128]{2,1,0:T(2,128)(2,1)} %param.24) | copy-start | bytes 3145732
  5.3 12.2 %copy-start.4 = (f32[2048]{0:T(1024)S(1)}, f32[2048]{0:T(1024)}, u32[]{:S(2)}) copy-start(f32[2048]{0:T(1024)} %param.21) | copy-start | bytes 24580
  5.3 12.7 %copy-start.2 = (f32[128]{0:T(128)S(1)}, f32[128]{0:T(128)}, u32[]{:S(2)}) copy-start(f32[128]{0:T(128)} %param.26) | copy-start | bytes 1540
